TPU v7x, 32 devices: a whole 2x2x4 slice. The times are simulated.
32 devices in a mesh: ep: 8 (over z, x), tp: 4 (over y, core).
Axes of the slice: x: 2, y: 2, z: 4, core: 2. Of those that a mesh axis runs over, the one named last changes fastest.
Arguments:
- tokens: bfloat16 [384, 1024], P('ep'), may hold values from -6 to 6
- head_state: float32 [384, 8, 64, 64], P('ep', 'tp'), may hold values from -6 to 6
- recept_weight: bfloat16 [1024, 512], P(None, 'tp'), may hold values from -0.1875 to 0.1875
- key_weight: bfloat16 [1024, 512], P(None, 'tp'), may hold values from -0.1875 to 0.1875
- value_weight: bfloat16 [1024, 512], P(None, 'tp'), may hold values from -0.1875 to 0.1875
- decay_down_factor: bfloat16 [1024, 64], replicated, may hold values from -0.1875 to 0.1875
- decay_up_factor: bfloat16 [64, 512], P(None, 'tp'), may hold values from -0.75 to 0.75
- decay_base: float32 [512], P('tp'), may hold values from -5 to 3
- rate_down_factor: bfloat16 [1024, 64], replicated, may hold values from -0.1875 to 0.1875
- rate_up_factor: bfloat16 [64, 512], P(None, 'tp'), may hold values from -0.75 to 0.75
- rate_base: float32 [512], P('tp'), may hold values from -3 to 3
- head_gain: float32 [512], P('tp'), may hold values from 0.1 to 1.9
- out_weight: bfloat16 [512, 1024], P('tp'), may hold values from -0.25 to 0.25
- route_experts: int32 [384, 4], P('ep'), may hold values from 0 to 7, all different within a row; in each aligned block of 48 rows (0 to 47, 48 to 95, ...) at most 48 rows name the same one
- route_weights: float32 [384, 4], P('ep'), may hold values from 0.03 to 0.2
- expert_gate: bfloat16 [8, 1024, 1024], P('ep', None, 'tp'), may hold values from -1 to 1
- expert_up: bfloat16 [8, 1024, 1024], P('ep', None, 'tp'), may hold values from -1 to 1
- expert_down: bfloat16 [8, 1024, 1024], P('ep', 'tp'), may hold values from -0.1875 to 0.1875
Outputs:
- layer_out: bfloat16 [384, 1024], P('ep', 'tp')
- new_state: float32 [384, 8, 64, 64], P('ep', 'tp')
Inputs may be any that keep to these rules, and one draw needn't show every extreme that they name: `route_experts`: each row names 4 different experts. In each aligned block of 48 rows no expert is named by more than 48 rows, a bound that some block reaches.
All inputs are finite; a program needn't handle non-finite values.
Results may differ from a plain program's by a relative error of at most 0.02.
Values may be sent and summed in bfloat16 or wider, within the bound.
A program may use at most 128 MiB of HBM per device.

v0:
```python
import functools

import jax
import jax.numpy as jnp
from jax import lax
from jax.experimental import pallas as pl
from jax.experimental.pallas import tpu as pltpu
from jax.sharding import PartitionSpec as P

NORM_EPS = 1e-05
GROUP_EPS = 0.00064
UNIT_EPS = 1e-06
CLAMP_LIMIT = 7.0
GLU_ALPHA = 1.702


MESH = pl.DeviceIdType.MESH
VMEM = pltpu.MemorySpace.VMEM


def row_norm(values):
    return values * lax.rsqrt(jnp.mean(values * values, axis=-1, keepdims=True) + NORM_EPS)


def clamped_unit(gate_pre, up_pre):
    gated = jnp.minimum(gate_pre, CLAMP_LIMIT)
    linear = jnp.clip(up_pre, -CLAMP_LIMIT, CLAMP_LIMIT)
    return gated * jax.nn.sigmoid(GLU_ALPHA * gated) * (linear + 1.0)


def heads_kernel(
    rows_per_step,
    tokens,
    state,
    recept_weight,
    key_weight,
    value_weight,
    decay_down,
    decay_up,
    decay_base,
    rate_down,
    rate_up,
    rate_base,
    gain,
    new_state,
    mixed,
    held,
    load_sem,
    store_sem,
    decay_rows,
    unit_rows,
    key_rows,
    value_rows,
    recept_rows,
    head_rows,
):
    seq_count, head_count, head_size = state.shape[:3]
    steps = seq_count // rows_per_step

    def chunk(step):
        return pl.ds(step * rows_per_step, rows_per_step)

    def load(step):
        return pltpu.make_async_copy(
            state.at[chunk(step)], held.at[chunk(step)], load_sem.at[step]
        )

    def store(step):
        return pltpu.make_async_copy(
            held.at[chunk(step)], new_state.at[chunk(step)], store_sem.at[step]
        )

    for step in range(steps):
        load(step).start()
    normed = row_norm(tokens[...].astype(jnp.float32)).astype(jnp.bfloat16)

    def product(left, right):
        return jnp.dot(left, right[...], preferred_element_type=jnp.float32)

    def turned(left, right):
        return lax.dot_general(
            left, right[...], (((1,), (1,)), ((), ())), preferred_element_type=jnp.float32
        )

    def rounded(value):
        return value.astype(jnp.bfloat16)

    recept = rounded(product(normed, recept_weight)).astype(jnp.float32)
    keys = rounded(product(normed, key_weight)).astype(jnp.float32)
    values = rounded(product(normed, value_weight)).astype(jnp.float32)
    decay_low = rounded(jnp.tanh(turned(normed, decay_down)))
    rate_low = rounded(turned(normed, rate_down))
    decay_pre = decay_base[...] + product(decay_low, decay_up)
    softplus = jnp.maximum(-decay_pre, 0.0) + jnp.log(1.0 + jnp.exp(-jnp.abs(decay_pre)))
    decay = jnp.exp(-jnp.exp(-softplus - 0.5))
    rate = jax.nn.sigmoid(rate_base[...] + product(rate_low, rate_up))
    for head in range(head_count):
        lanes = slice(head * head_size, (head + 1) * head_size)
        head_keys = keys[:, lanes]
        scale = lax.rsqrt(jnp.sum(head_keys * head_keys, axis=-1, keepdims=True) + UNIT_EPS)
        decay_rows[head] = decay[:, lanes]
        unit_rows[head] = head_keys * scale * scale
        key_rows[head] = head_keys * rate[:, lanes]
        value_rows[head] = values[:, lanes]
        recept_rows[head] = recept[:, lanes]

    shape = (head_size, head_size)
    diagonal = lax.broadcasted_iota(jnp.int32, shape, 0) == lax.broadcasted_iota(jnp.int32, shape, 1)

    ones = jnp.ones(shape, jnp.bfloat16)

    def lane_sums(blocks):
        block = jnp.concatenate(blocks, axis=0)
        high = block.astype(jnp.bfloat16)
        low = (block - high.astype(jnp.float32)).astype(jnp.bfloat16)
        sums = jnp.dot(high, ones, preferred_element_type=jnp.float32)
        sums += jnp.dot(low, ones, preferred_element_type=jnp.float32)
        return [sums[i * head_size : (i + 1) * head_size] for i in range(len(blocks))]

    def advance(step, _):
        load(step).wait()
        for index in range(0, rows_per_step, 2):
            pairs = [
                (step * rows_per_step + index + extra, head)
                for extra in range(min(2, rows_per_step - index))
                for head in range(head_count)
            ]
            olds = [held[pair] for pair in pairs]
            pulled = []
            for (seq, head), old in zip(pairs, olds):
                row = pl.ds(seq, 1)
                values = jnp.where(diagonal, value_rows[head, row, :], 0.0)
                pulled.append(values - old * unit_rows[head, row, :])
            columns = lane_sums(pulled)
            weighted = []
            for (seq, head), old, column in zip(pairs, olds, columns):
                row = pl.ds(seq, 1)
                fresh = old * decay_rows[head, row, :] + column * key_rows[head, row, :]
                held[seq, head] = fresh
                weighted.append(fresh * recept_rows[head, row, :])
            for (seq, head), outs in zip(pairs, lane_sums(weighted)):
                outs = jnp.sum(jnp.where(diagonal, outs, 0.0), axis=0, keepdims=True)
                head_rows[head, pl.ds(seq, 1), :] = outs
        store(step).start()
        return 0

    lax.fori_loop(0, steps, advance, 0)
    for head in range(head_count):
        outs = head_rows[head]
        centred = outs - jnp.mean(outs, axis=-1, keepdims=True)
        spread = jnp.mean(centred * centred, axis=-1, keepdims=True)
        lanes = slice(head * head_size, (head + 1) * head_size)
        mixed[head] = centred * lax.rsqrt(spread + GROUP_EPS) * gain[:, lanes]
    for step in range(steps):
        store(step).wait()


def run_heads(tokens, head_state, *parameters):
    seq_count, head_count, head_size = head_state.shape[:3]
    rows_per_step = 8 if seq_count % 8 == 0 else seq_count
    parameters = [each.reshape(1, -1) if each.ndim == 1 else each for each in parameters]

    rows = (head_count, seq_count, head_size)
    vmem = pl.BlockSpec(memory_space=VMEM)
    anywhere = pl.BlockSpec(memory_space=pltpu.MemorySpace.HBM)
    steps = seq_count // rows_per_step
    return pl.pallas_call(
        functools.partial(heads_kernel, rows_per_step),
        in_specs=[vmem, anywhere] + [vmem] * len(parameters),
        out_specs=[anywhere, vmem],
        out_shape=[
            jax.ShapeDtypeStruct(head_state.shape, jnp.float32),
            jax.ShapeDtypeStruct(rows, jnp.float32),
        ],
        scratch_shapes=[
            pltpu.VMEM(head_state.shape, jnp.float32),
            pltpu.SemaphoreType.DMA((steps,)),
            pltpu.SemaphoreType.DMA((steps,)),
        ]
        + [pltpu.VMEM(rows, jnp.float32)] * 6,
        name="heads",
    )(tokens, head_state, *parameters)


def flipped(index, mask):
    bit = 1
    result = index
    while bit <= mask:
        if mask & bit:
            result = result + bit * (1 - 2 * ((index // bit) % 2))
        bit *= 2
    return result


def experts_kernel(
    n_ep,
    n_tp,
    mixed,
    out_weight,
    tokens,
    routes,
    weights,
    gate_hbm,
    up_hbm,
    down_hbm,
    layer_out,
    gate,
    up,
    down,
    shares,
    got_shares,
    rows,
    parts,
    leaving,
    arriving,
    homeward,
    returned,
    weight_sem,
    share_send,
    share_recv,
    spread_send,
    rows_send,
    rows_recv,
    part_send,
    part_recv,
    home_send,
    home_recv,
):
    me_ep, me_tp = lax.axis_index("ep"), lax.axis_index("tp")
    seq_count = tokens.shape[0]
    columns = shares.shape[2]
    head_count, _, head_size = mixed.shape
    levels = n_tp.bit_length() - 1

    barrier = pltpu.get_barrier_semaphore()
    for mask in range(1, n_tp):
        pl.semaphore_signal(
            barrier, inc=1, device_id={"tp": flipped(me_tp, mask)}, device_id_type=MESH
        )
    for mask in range(1, n_ep):
        pl.semaphore_signal(
            barrier, inc=1, device_id={"ep": flipped(me_ep, mask)}, device_id_type=MESH
        )
    loads = [
        pltpu.make_async_copy(source.at[0], target, weight_sem.at[index])
        for index, (source, target) in enumerate(((gate_hbm, gate), (up_hbm, up), (down_hbm, down)))
    ]
    for load in loads:
        load.start()
    started = []

    def send(source, target, send_sem, recv_sem, device):
        copy = pltpu.make_async_remote_copy(
            src_ref=source,
            dst_ref=target,
            send_sem=send_sem,
            recv_sem=recv_sem,
            device_id=device,
            device_id_type=MESH,
        )
        copy.start()
        started.append(copy)
        return copy

    projected = jnp.zeros((seq_count, out_weight.shape[1]), jnp.float32)
    for head in range(head_count):
        projected += jnp.dot(
            mixed[head].astype(jnp.bfloat16),
            out_weight[head * head_size : (head + 1) * head_size, :],
            preferred_element_type=jnp.float32,
        )
    for part in range(n_tp):
        shares[part] = projected[:, part * columns : (part + 1) * columns].astype(jnp.bfloat16)
    pl.semaphore_wait(barrier, n_tp + n_ep - 2)

    incoming = [
        send(
            shares.at[flipped(me_tp, mask)],
            got_shares.at[mask - 1],
            share_send.at[mask - 1],
            share_recv.at[mask - 1],
            {"tp": flipped(me_tp, mask)},
        )
        for mask in range(n_tp - 1, 0, -1)
    ]
    own_columns = pl.ds(pl.multiple_of(me_tp * columns, columns), columns)
    summed = shares[me_tp].astype(jnp.float32)
    for copy in incoming:
        copy.wait_recv()
    for mask in range(1, n_tp):
        summed += got_shares[mask - 1].astype(jnp.float32)
    residual = (tokens[:, own_columns].astype(jnp.float32) + summed).astype(jnp.bfloat16)
    rows[0, 0] = residual

    got = {}
    for mask in range(n_ep - 1, 0, -1):
        got[mask, 0] = send(
            rows.at[0, 0],
            rows.at[mask, 0],
            spread_send.at[mask - 1],
            rows_recv.at[mask, 0],
            {"ep": flipped(me_ep, mask)},
        )

    def forward(mask, part, bit):
        got[mask, part + bit] = send(
            rows.at[mask, part],
            rows.at[mask, part + bit],
            rows_send.at[mask, part + bit],
            rows_recv.at[mask, part + bit],
            {"tp": flipped(me_tp, bit)},
        )

    bits = [1 << level for level in range(levels - 1, -1, -1)]
    for mask in range(n_ep):
        if mask:
            got[mask, 0].wait_recv()
        for bit in bits:
            forward(mask, 0, bit)

    def relay(masks):
        for top in bits[:-1]:
            for part in range(top, n_tp, 2 * top):
                for mask in masks:
                    got[mask, part].wait_recv()
                    for bit in bits:
                        if bit < top:
                            forward(mask, part, bit)

    near, far = range(n_ep // 2), range(n_ep // 2, n_ep)
    copies = {}

    def own(part):
        return pl.ds(pl.multiple_of(flipped(me_tp, part) * columns, columns), columns)

    def send_part(part, mask, bit):
        copies[part, mask] = send(
            leaving.at[part, mask],
            arriving.at[part, mask],
            part_send.at[part, mask],
            part_recv.at[part, mask],
            {"tp": flipped(me_tp, bit)},
        )

    def compute(masks):
        for mask in masks:
            for part in range(1, n_tp, 2):
                got[mask, part].wait_recv()
        span = slice(masks[0], masks[-1] + 1)
        total = len(masks) * seq_count
        squares = jnp.zeros((total, columns), jnp.float32)
        gate_pre = jnp.zeros((total, gate.shape[1]), jnp.float32)
        up_pre = jnp.zeros((total, up.shape[1]), jnp.float32)
        for part in range(n_tp):
            block = rows[span, part].reshape(total, columns)
            wide = block.astype(jnp.float32)
            squares += wide * wide
            gate_pre += jnp.dot(block, gate[own(part), :], preferred_element_type=jnp.float32)
            up_pre += jnp.dot(block, up[own(part), :], preferred_element_type=jnp.float32)
        mean = jnp.sum(squares, axis=-1, keepdims=True) / (n_tp * columns)
        scale = lax.rsqrt(mean + NORM_EPS)
        activated = clamped_unit(gate_pre * scale, up_pre * scale).astype(jnp.bfloat16)
        shape = (len(masks), seq_count, columns)
        for part in list(range(1, n_tp, 2)) + list(range(0, n_tp, 2)):
            value = jnp.dot(activated, down[:, own(part)], preferred_element_type=jnp.float32)
            if part % 2 == 0:
                parts[part, span] = value.reshape(shape)
                continue
            leaving[part, span] = value.astype(jnp.bfloat16).reshape(shape)
            for mask in reversed(masks):
                send_part(part, mask, 1)

    def fold(masks):
        for level in range(1, levels):
            bit = 1 << level
            for mask in reversed(masks):
                for part in range(n_tp - bit, -1, -bit):
                    before = part + bit // 2
                    copies[before, mask].wait_recv()
                    value = parts[part, mask] + arriving[before, mask].astype(jnp.float32)
                    if part % (2 * bit) == bit:
                        leaving[part, mask] = value.astype(jnp.bfloat16)
                        send_part(part, mask, bit)
                    else:
                        parts[part, mask] = value

    back = {}

    def home(masks):
        for mask in reversed(masks):
            last = n_tp // 2
            copies[last, mask].wait_recv()
            value = (parts[0, mask] + arriving[last, mask].astype(jnp.float32)).astype(jnp.bfloat16)
            if mask == 0:
                returned[0] = value
                continue
            homeward[mask - 1] = value
            back[mask] = send(
                homeward.at[mask - 1],
                returned.at[mask],
                home_send.at[mask - 1],
                home_recv.at[mask - 1],
                {"ep": flipped(me_ep, mask)},
            )

    relay(near)
    for load in loads:
        load.wait()
    compute(near)
    relay(far)
    fold(near)
    compute(far)
    fold(far)
    home(near)
    home(far)
    shape = (seq_count, seq_count)
    diagonal = lax.broadcasted_iota(jnp.int32, shape, 0) == lax.broadcasted_iota(jnp.int32, shape, 1)
    result = residual.astype(jnp.float32)
    for mask in range(n_ep):
        chosen = routes[...] == flipped(me_ep, mask)
        share = jnp.sum(jnp.where(chosen, weights[...], 0.0), axis=0, keepdims=True)
        share = jnp.sum(jnp.where(diagonal, share, 0.0), axis=-1, keepdims=True)
        if mask:
            back[mask].wait_recv()
        result += share * returned[mask].astype(jnp.float32)
    layer_out[...] = result
    for copy in started:
        copy.wait_send()


def run_experts(mixed, out_weight, tokens, routes, weights, gate, up, down):
    n_ep, n_tp = lax.axis_size("ep"), lax.axis_size("tp")
    seq_count, width = tokens.shape
    columns = width // n_tp
    block = (seq_count, columns)
    vmem = pl.BlockSpec(memory_space=VMEM)
    anywhere = pl.BlockSpec(memory_space=pl.ANY)
    dma = pltpu.SemaphoreType.DMA
    return pl.pallas_call(
        functools.partial(experts_kernel, n_ep, n_tp),
        in_specs=[vmem] * 5 + [anywhere] * 3,
        out_specs=vmem,
        out_shape=jax.ShapeDtypeStruct(block, jnp.float32),
        scratch_shapes=[
            pltpu.VMEM(gate.shape[1:], jnp.bfloat16),
            pltpu.VMEM(up.shape[1:], jnp.bfloat16),
            pltpu.VMEM(down.shape[1:], jnp.bfloat16),
            pltpu.VMEM((n_tp,) + block, jnp.bfloat16),
            pltpu.VMEM((n_tp - 1,) + block, jnp.bfloat16),
            pltpu.VMEM((n_ep, n_tp) + block, jnp.bfloat16),
            pltpu.VMEM((n_tp, n_ep) + block, jnp.float32),
            pltpu.VMEM((n_tp, n_ep) + block, jnp.bfloat16),
            pltpu.VMEM((n_tp, n_ep) + block, jnp.bfloat16),
            pltpu.VMEM((n_ep - 1,) + block, jnp.bfloat16),
            pltpu.VMEM((n_ep,) + block, jnp.bfloat16),
            dma((3,)),
            dma((n_tp - 1,)),
            dma((n_tp - 1,)),
            dma((n_ep - 1,)),
            dma((n_ep, n_tp)),
            dma((n_ep, n_tp)),
            dma((n_tp, n_ep)),
            dma((n_tp, n_ep)),
            dma((n_ep - 1,)),
            dma((n_ep - 1,)),
        ],
        compiler_params=pltpu.CompilerParams(collective_id=0, has_side_effects=True),
        name="experts",
    )(mixed, out_weight, tokens, routes, weights, gate, up, down).astype(jnp.bfloat16)


def every_row_fits(seq_count, top_count, width):
    n_ep, n_tp = lax.axis_size("ep"), lax.axis_size("tp")
    capacity = max(2, (2 * seq_count * top_count + n_ep - 1) // n_ep)
    powers = n_ep & (n_ep - 1) == 0 and n_tp & (n_tp - 1) == 0 and min(n_ep, n_tp) > 1
    aligned = seq_count % 16 == 0 and width % (128 * n_tp) == 0
    return capacity >= seq_count and powers and aligned


def local(
    tokens,
    head_state,
    recept_weight,
    key_weight,
    value_weight,
    decay_down_factor,
    decay_up_factor,
    decay_base,
    rate_down_factor,
    rate_up_factor,
    rate_base,
    head_gain,
    out_weight,
    route_experts,
    route_weights,
    expert_gate,
    expert_up,
    expert_down,
):
    new_state, mixed = run_heads(
        tokens,
        head_state,
        recept_weight,
        key_weight,
        value_weight,
        decay_down_factor.T,
        decay_up_factor,
        decay_base,
        rate_down_factor.T,
        rate_up_factor,
        rate_base,
        head_gain,
    )
    if every_row_fits(*route_experts.shape, tokens.shape[1]):
        layer_out = run_experts(
            mixed,
            out_weight,
            tokens,
            route_experts.T,
            route_weights.T,
            expert_gate,
            expert_up,
            expert_down,
        )
        return (layer_out, new_state)
    mixed = jnp.swapaxes(mixed, 0, 1).reshape(tokens.shape[0], -1).astype(jnp.bfloat16)
    tokens_float = tokens.astype(jnp.float32)
    partial_value = jnp.dot(mixed, out_weight, preferred_element_type=jnp.float32).astype(
        jnp.bfloat16
    )
    partial_value = lax.optimization_barrier(partial_value).astype(jnp.float32)
    summed = lax.psum(partial_value.astype(jnp.bfloat16), "tp").astype(jnp.float32)
    residual = (tokens_float + summed).astype(jnp.bfloat16)
    expert_input = row_norm(residual.astype(jnp.float32)).astype(jnp.bfloat16)
    seq_count, top_count = route_experts.shape
    expert_count = lax.axis_size("ep")
    capacity = max(2, (2 * seq_count * top_count + expert_count - 1) // expert_count)
    column_count = expert_input.shape[1] // lax.axis_size("tp")
    column_start = lax.axis_index("tp") * column_count
    flat_routes = route_experts.reshape(-1)
    onehot = (flat_routes[:, None] == jnp.arange(expert_count, dtype=jnp.int32)[None, :]).astype(
        jnp.int32
    )
    earlier = jnp.cumsum(onehot, axis=0) - onehot
    target = flat_routes * capacity + jnp.sum(earlier * onehot, axis=1)
    slot_ids = jnp.arange(expert_count * capacity, dtype=jnp.int32)
    dispatch_map = jnp.any(
        slot_ids[:, None, None] == target.reshape(seq_count, top_count)[None], axis=-1
    )
    dispatch_map = dispatch_map.astype(jnp.bfloat16)
    outgoing = lax.dynamic_slice_in_dim(expert_input, column_start, column_count, 1)
    buffer = jnp.dot(dispatch_map, outgoing, preferred_element_type=jnp.float32).astype(
        jnp.bfloat16
    )
    buffer = buffer.reshape(expert_count, capacity, outgoing.shape[1])
    slot_rows = lax.all_gather(
        lax.all_to_all(buffer, "ep", split_axis=0, concat_axis=0, tiled=True),
        "tp",
        axis=2,
        tiled=True,
    )
    source_count, slot_count, model_width = slot_rows.shape
    flat_rows = slot_rows.reshape(-1, model_width)
    gate_pre = jnp.dot(flat_rows, expert_gate[0], preferred_element_type=jnp.float32)
    up_pre = jnp.dot(flat_rows, expert_up[0], preferred_element_type=jnp.float32)
    activated = clamped_unit(gate_pre, up_pre).astype(jnp.bfloat16)
    part_out = jnp.dot(activated, expert_down[0], preferred_element_type=jnp.float32).astype(
        jnp.bfloat16
    )
    part_out = lax.optimization_barrier(part_out).astype(jnp.float32)
    part_out = part_out.reshape(source_count, slot_count, model_width)
    shares = lax.psum_scatter(part_out.astype(jnp.bfloat16), "tp", scatter_dimension=2, tiled=True)
    returned = lax.all_to_all(shares, "ep", split_axis=0, concat_axis=0, tiled=True)
    picked = returned.reshape(expert_count * capacity, column_count)[target]
    picked = picked.reshape(seq_count, top_count, column_count).astype(jnp.float32)
    mixture = jnp.sum(route_weights[:, :, None] * picked, axis=1)
    own_residual = lax.dynamic_slice_in_dim(residual, column_start, column_count, 1).astype(
        jnp.float32
    )
    layer_out = (own_residual + mixture).astype(jnp.bfloat16)
    return (layer_out, new_state)


def solution(mesh):
    in_specs = (
        P("ep", None),
        P("ep", "tp", None, None),
        P(None, "tp"),
        P(None, "tp"),
        P(None, "tp"),
        P(),
        P(None, "tp"),
        P("tp"),
        P(),
        P(None, "tp"),
        P("tp"),
        P("tp"),
        P("tp", None),
        P("ep", None),
        P("ep", None),
        P("ep", None, "tp"),
        P("ep", None, "tp"),
        P("ep", "tp", None),
    )
    out_specs = (P("ep", "tp"), P("ep", "tp", None, None))
    return jax.shard_map(local, mesh=mesh, in_specs=in_specs, out_specs=out_specs, check_vma=False)
```

profile of v0, /device:TPU:0, one launch (start us, length us, event | category | flops | bytes accessed | tf_op | source)
XLA Modules:
  0.0 42.6 jit_solution(17389859804700448708)
XLA Ops:
  0.6 7.1 %heads.1 = (f32[48,2,64,64]{3,2,1,0:T(8,128)}, f32[2,48,64]{2,1,0:T(8,128)}) custom-call(bf16[48,1024]{1,0:T(8,128)(2,1)} %tokens.3, f32[48,2,64,64]{3,2,1,0:T(8,128)} %state.1, bf16[1024,128]{1,0:T(8,128)(2,1)} %recept_weight.1, bf16[1024,128]{1,0:T(8,128)(2,1)} %key_weight.1, bf16[1024,128]{1,0:T(8,128)(2,1)} %value_weight.1, bf16[64,1024]{1,0:T(8,128)(2,1)} %bitcast.7, ...), custom_call_target="tpu_custom_call" | custom-call | tf_op jit(solution)/shard_map/heads/pallas_call | solution.py:167
  7.7 33.5 %experts.1 = f32[48,256]{1,0:T(8,128)} custom-call(f32[2,48,64]{2,1,0:T(8,128)} %get-tuple-element.4.mixed, bf16[128,1024]{1,0:T(8,128)(2,1)} %out_weight.1, bf16[48,1024]{1,0:T(8,128)(2,1)} %tokens.3, s32[4,48]{1,0:T(4,128)} %bitcast.9, f32[4,48]{1,0:T(4,128)} %bitcast.10, bf16[1,1024,256]{2,1,0:T(8,128)(2,1)} %gate_hbm.1, bf16[1,1024,256]{2,1,0:T(8,128)(2,1)} %up_hbm.1, ...), custom_call_target="tpu_custom_call" | custom-call | tf_op jit(solution)/shard_map/experts/pallas_call | solution.py:439
  41.2 1.4 %convert_element_type.3 = bf16[48,256]{1,0:T(8,128)(2,1)} convert(f32[48,256]{1,0:T(8,128)} %experts.1) | non-fusion elementwise | flops 12288 | bytes 73728 | tf_op jit(solution)/shard_map/convert_element_type | solution.py:469
where the time goes:
time: 42.8 us; the launch traced here: 42.6 us
  Pallas kernels  40.5 us (95%)
  other arithmetic  1.41 us (3%)
  between operations  0.65 us (2%)
    pallas_call x1, Pallas kernels, run_experts(): pl.pallas_call(functools.partial(experts_kernel, n_ep, n_tp), in_specs=[v...  33.5 us
    pallas_call x1, Pallas kernels, run_heads(): pl.pallas_call(functools.partial(heads_kernel, rows_per_step), in_specs=[...  7.09 us
    convert_element_type x1, other arithmetic, run_experts(): return pl.pallas_call(functools.partial(experts_kernel, n_ep, n_tp), in_s...  1.41 us

commit v1 on v0

--- a/solution.py
+++ b/solution.py
@@ -28,32 +28,14 @@
     return gated * jax.nn.sigmoid(GLU_ALPHA * gated) * (linear + 1.0)
 
 
-def heads_kernel(
-    rows_per_step,
-    tokens,
-    state,
-    recept_weight,
-    key_weight,
-    value_weight,
-    decay_down,
-    decay_up,
-    decay_base,
-    rate_down,
-    rate_up,
-    rate_base,
-    gain,
-    new_state,
-    mixed,
-    held,
-    load_sem,
-    store_sem,
-    decay_rows,
-    unit_rows,
-    key_rows,
-    value_rows,
-    recept_rows,
-    head_rows,
-):
+def heads_kernel(rows_per_step, input_count, *refs):
+    state, inputs = refs[0], refs[1 : 1 + input_count]
+    new_state, mixed, held = refs[1 + input_count : 4 + input_count]
+    copies = refs[4 + input_count : 4 + 2 * input_count]
+    input_sem, load_sem, store_sem, decay_rows, unit_rows, key_rows = refs[
+        4 + 2 * input_count : 10 + 2 * input_count
+    ]
+    value_rows, recept_rows, head_rows = refs[10 + 2 * input_count :]
     seq_count, head_count, head_size = state.shape[:3]
     steps = seq_count // rows_per_step
 
@@ -70,8 +52,29 @@
             held.at[chunk(step)], new_state.at[chunk(step)], store_sem.at[step]
         )
 
+    staged = [
+        pltpu.make_async_copy(source, target, input_sem.at[index])
+        for index, (source, target) in enumerate(zip(inputs, copies))
+    ]
+    for copy in staged:
+        copy.start()
+    for copy in staged:
+        copy.wait()
     for step in range(steps):
         load(step).start()
+    (
+        tokens,
+        recept_weight,
+        key_weight,
+        value_weight,
+        decay_down,
+        decay_up,
+        decay_base,
+        rate_down,
+        rate_up,
+        rate_base,
+        gain,
+    ) = copies
     normed = row_norm(tokens[...].astype(jnp.float32)).astype(jnp.bfloat16)
 
     def product(left, right):
@@ -79,7 +82,7 @@
 
     def turned(left, right):
         return lax.dot_general(
-            left, right[...], (((1,), (1,)), ((), ())), preferred_element_type=jnp.float32
+            left, right, (((1,), (1,)), ((), ())), preferred_element_type=jnp.float32
         )
 
     def rounded(value):
@@ -88,8 +91,8 @@
     recept = rounded(product(normed, recept_weight)).astype(jnp.float32)
     keys = rounded(product(normed, key_weight)).astype(jnp.float32)
     values = rounded(product(normed, value_weight)).astype(jnp.float32)
-    decay_low = rounded(jnp.tanh(turned(normed, decay_down)))
-    rate_low = rounded(turned(normed, rate_down))
+    decay_low = rounded(jnp.tanh(turned(normed, decay_down[...])))
+    rate_low = rounded(turned(normed, rate_down[...]))
     decay_pre = decay_base[...] + product(decay_low, decay_up)
     softplus = jnp.maximum(-decay_pre, 0.0) + jnp.log(1.0 + jnp.exp(-jnp.abs(decay_pre)))
     decay = jnp.exp(-jnp.exp(-softplus - 0.5))
@@ -106,80 +109,81 @@
 
     shape = (head_size, head_size)
     diagonal = lax.broadcasted_iota(jnp.int32, shape, 0) == lax.broadcasted_iota(jnp.int32, shape, 1)
-
     ones = jnp.ones(shape, jnp.bfloat16)
-
-    def lane_sums(blocks):
-        block = jnp.concatenate(blocks, axis=0)
-        high = block.astype(jnp.bfloat16)
-        low = (block - high.astype(jnp.float32)).astype(jnp.bfloat16)
-        sums = jnp.dot(high, ones, preferred_element_type=jnp.float32)
-        sums += jnp.dot(low, ones, preferred_element_type=jnp.float32)
-        return [sums[i * head_size : (i + 1) * head_size] for i in range(len(blocks))]
+    places = lax.broadcasted_iota(jnp.int32, (rows_per_step, head_size), 0)
+    width = next(each for each in (4, 2, 1) if rows_per_step % each == 0)
 
     def advance(step, _):
         load(step).wait()
-        for index in range(0, rows_per_step, 2):
-            pairs = [
-                (step * rows_per_step + index + extra, head)
-                for extra in range(min(2, rows_per_step - index))
-                for head in range(head_count)
-            ]
-            olds = [held[pair] for pair in pairs]
-            pulled = []
-            for (seq, head), old in zip(pairs, olds):
-                row = pl.ds(seq, 1)
-                values = jnp.where(diagonal, value_rows[head, row, :], 0.0)
-                pulled.append(values - old * unit_rows[head, row, :])
-            columns = lane_sums(pulled)
-            weighted = []
-            for (seq, head), old, column in zip(pairs, olds, columns):
-                row = pl.ds(seq, 1)
-                fresh = old * decay_rows[head, row, :] + column * key_rows[head, row, :]
-                held[seq, head] = fresh
-                weighted.append(fresh * recept_rows[head, row, :])
-            for (seq, head), outs in zip(pairs, lane_sums(weighted)):
-                outs = jnp.sum(jnp.where(diagonal, outs, 0.0), axis=0, keepdims=True)
-                head_rows[head, pl.ds(seq, 1), :] = outs
+        for head in range(head_count):
+            queries = rounded(recept_rows[head, chunk(step), :])
+            total = jnp.zeros((rows_per_step, head_size), jnp.float32)
+            for first in range(0, rows_per_step, width):
+                seqs = [step * rows_per_step + first + each for each in range(width)]
+                olds = [held[seq, head] for seq in seqs]
+                pulled = []
+                for seq, old in zip(seqs, olds):
+                    row = pl.ds(seq, 1)
+                    wanted = jnp.where(diagonal, value_rows[head, row, :], 0.0)
+                    pulled.append(rounded(wanted - old * unit_rows[head, row, :]))
+                columns = product(jnp.concatenate(pulled, axis=0), ones)
+                blocks = []
+                for each, (seq, old) in enumerate(zip(seqs, olds)):
+                    row = pl.ds(seq, 1)
+                    column = columns[each * head_size : (each + 1) * head_size]
+                    fresh = old * decay_rows[head, row, :] + column * key_rows[head, row, :]
+                    held[seq, head] = fresh
+                    blocks.append(rounded(fresh * recept_rows[head, row, :]))
+                outs = product(jnp.concatenate(blocks, axis=0), ones)
+                for each, seq in enumerate(seqs):
+                    part = outs[each * head_size : (each + 1) * head_size]
+                    part = jnp.sum(jnp.where(diagonal, part, 0.0), axis=0, keepdims=True)
+                    head_rows[head, pl.ds(seq, 1), :] = part
         store(step).start()
         return 0
 
     lax.fori_loop(0, steps, advance, 0)
+    wide = []
     for head in range(head_count):
         outs = head_rows[head]
         centred = outs - jnp.mean(outs, axis=-1, keepdims=True)
         spread = jnp.mean(centred * centred, axis=-1, keepdims=True)
         lanes = slice(head * head_size, (head + 1) * head_size)
-        mixed[head] = centred * lax.rsqrt(spread + GROUP_EPS) * gain[:, lanes]
+        wide.append(centred * lax.rsqrt(spread + GROUP_EPS) * gain[:, lanes])
+    mixed[...] = rounded(jnp.concatenate(wide, axis=-1))
     for step in range(steps):
         store(step).wait()
+
+
+def in_hbm(value):
+    return pltpu.with_memory_space_constraint(value, pltpu.MemorySpace.HBM)
 
 
 def run_heads(tokens, head_state, *parameters):
     seq_count, head_count, head_size = head_state.shape[:3]
     rows_per_step = 8 if seq_count % 8 == 0 else seq_count
-    parameters = [each.reshape(1, -1) if each.ndim == 1 else each for each in parameters]
+    inputs = [tokens] + [each.reshape(1, -1) if each.ndim == 1 else each for each in parameters]
 
     rows = (head_count, seq_count, head_size)
-    vmem = pl.BlockSpec(memory_space=VMEM)
+    mixed = (seq_count, head_count * head_size)
     anywhere = pl.BlockSpec(memory_space=pltpu.MemorySpace.HBM)
     steps = seq_count // rows_per_step
+    dma = pltpu.SemaphoreType.DMA
     return pl.pallas_call(
-        functools.partial(heads_kernel, rows_per_step),
-        in_specs=[vmem, anywhere] + [vmem] * len(parameters),
-        out_specs=[anywhere, vmem],
+        functools.partial(heads_kernel, rows_per_step, len(inputs)),
+        in_specs=[anywhere] * (1 + len(inputs)),
+        out_specs=[anywhere, pl.BlockSpec(memory_space=VMEM)],
         out_shape=[
-            jax.ShapeDtypeStruct(head_state.shape, jnp.float32),
-            jax.ShapeDtypeStruct(rows, jnp.float32),
+            pltpu.MemorySpace.HBM(head_state.shape, jnp.float32),
+            VMEM(mixed, jnp.bfloat16),
         ],
-        scratch_shapes=[
-            pltpu.VMEM(head_state.shape, jnp.float32),
-            pltpu.SemaphoreType.DMA((steps,)),
-            pltpu.SemaphoreType.DMA((steps,)),
-        ]
+        scratch_shapes=[pltpu.VMEM(head_state.shape, jnp.float32)]
+        + [pltpu.VMEM(each.shape, each.dtype) for each in inputs]
+        + [dma((len(inputs),)), dma((steps,)), dma((steps,))]
         + [pltpu.VMEM(rows, jnp.float32)] * 6,
+        compiler_params=pltpu.CompilerParams(vmem_limit_bytes=40 * 2**20),
         name="heads",
-    )(tokens, head_state, *parameters)
+    )(*map(in_hbm, [head_state] + inputs))
 
 
 def flipped(index, mask):
@@ -229,7 +233,6 @@
     me_ep, me_tp = lax.axis_index("ep"), lax.axis_index("tp")
     seq_count = tokens.shape[0]
     columns = shares.shape[2]
-    head_count, _, head_size = mixed.shape
     levels = n_tp.bit_length() - 1
 
     barrier = pltpu.get_barrier_semaphore()
@@ -262,13 +265,7 @@
         started.append(copy)
         return copy
 
-    projected = jnp.zeros((seq_count, out_weight.shape[1]), jnp.float32)
-    for head in range(head_count):
-        projected += jnp.dot(
-            mixed[head].astype(jnp.bfloat16),
-            out_weight[head * head_size : (head + 1) * head_size, :],
-            preferred_element_type=jnp.float32,
-        )
+    projected = jnp.dot(mixed[...], out_weight[...], preferred_element_type=jnp.float32)
     for part in range(n_tp):
         shares[part] = projected[:, part * columns : (part + 1) * columns].astype(jnp.bfloat16)
     pl.semaphore_wait(barrier, n_tp + n_ep - 2)
@@ -440,7 +437,7 @@
         functools.partial(experts_kernel, n_ep, n_tp),
         in_specs=[vmem] * 5 + [anywhere] * 3,
         out_specs=vmem,
-        out_shape=jax.ShapeDtypeStruct(block, jnp.float32),
+        out_shape=VMEM(block, jnp.float32),
         scratch_shapes=[
             pltpu.VMEM(gate.shape[1:], jnp.bfloat16),
             pltpu.VMEM(up.shape[1:], jnp.bfloat16),
@@ -464,9 +461,9 @@
             dma((n_ep - 1,)),
             dma((n_ep - 1,)),
         ],
-        compiler_params=pltpu.CompilerParams(collective_id=0, has_side_effects=True),
+        compiler_params=pltpu.CompilerParams(collective_id=0, has_side_effects=True, vmem_limit_bytes=40 * 2**20),
         name="experts",
-    )(mixed, out_weight, tokens, routes, weights, gate, up, down).astype(jnp.bfloat16)
+    )(mixed, *map(in_hbm, (out_weight, tokens, routes, weights, gate, up, down))).astype(jnp.bfloat16)
 
 
 def every_row_fits(seq_count, top_count, width):
@@ -523,7 +520,6 @@
             expert_down,
         )
         return (layer_out, new_state)
-    mixed = jnp.swapaxes(mixed, 0, 1).reshape(tokens.shape[0], -1).astype(jnp.bfloat16)
     tokens_float = tokens.astype(jnp.float32)
     partial_value = jnp.dot(mixed, out_weight, preferred_element_type=jnp.float32).astype(
         jnp.bfloat16

time: 42.8 us -> 39.8 us (0.930)
  Pallas kernels: 40.5 us -> 38.4 us
  other arithmetic: 1.41 us -> 0.61 us
    pallas_call x1, Pallas kernels: 7.09 us -> 5.54 us  [run_heads(): pl.pallas_call(functools.partial(heads_kernel, rows_per_step, len(inputs)...]
    convert_element_type x1, other arithmetic: 1.41 us -> 0.61 us  [run_experts(): return pl.pallas_call(functools.partial(experts_kernel, n_ep, n_tp), in_s...]
    pallas_call x1, Pallas kernels: 33.5 us -> 32.8 us  [run_experts(): pl.pallas_call(functools.partial(experts_kernel, n_ep, n_tp), in_specs=[v...]
where the time goes in v1:
time: 39.8 us; the launch traced here: 39.6 us
  Pallas kernels  38.4 us (96%)
  between operations  0.65 us (2%)
  other arithmetic  0.61 us (2%)
    pallas_call x1, Pallas kernels, run_experts(): pl.pallas_call(functools.partial(experts_kernel, n_ep, n_tp), in_specs=[v...  32.8 us
    pallas_call x1, Pallas kernels, run_heads(): pl.pallas_call(functools.partial(heads_kernel, rows_per_step, len(inputs)...  5.54 us

profile of v1, /device:TPU:0, one launch (start us, length us, event | category | flops | bytes accessed | tf_op | source)
XLA Modules:
  0.0 39.6 jit_solution(5327716253281972595)
XLA Ops:
  0.6 5.5 %heads.1 = (f32[48,2,64,64]{3,2,1,0:T(8,128)}, bf16[48,128]{1,0:T(8,128)(2,1)S(1)}) custom-call(f32[48,2,64,64]{3,2,1,0:T(8,128)} %refs_0_.1, bf16[48,1024]{1,0:T(8,128)(2,1)} %tokens.1, bf16[1024,128]{1,0:T(8,128)(2,1)} %refs_2_.1, bf16[1024,128]{1,0:T(8,128)(2,1)} %refs_3_.1, bf16[1024,128]{1,0:T(8,128)(2,1)} %refs_4_.1, bf16[64,1024]{1,0:T(8,128)(2,1)} %bitcast.7, ...), custom_call_target="tpu_custom_call" | custom-call | tf_op jit(solution)/shard_map/heads/pallas_call | solution.py:172
  6.2 32.8 %experts.1 = f32[48,256]{1,0:T(8,128)S(1)} custom-call(bf16[48,128]{1,0:T(8,128)(2,1)S(1)} %get-tuple-element.4.mixed, bf16[128,1024]{1,0:T(8,128)(2,1)} %out_weight.1, bf16[48,1024]{1,0:T(8,128)(2,1)} %tokens.1, s32[4,48]{1,0:T(4,128)} %bitcast.9, f32[4,48]{1,0:T(4,128)} %bitcast.10, bf16[1,1024,256]{2,1,0:T(8,128)(2,1)} %gate_hbm.1, ...), custom_call_target="tpu_custom_call" | custom-call | tf_op jit(solution)/shard_map/experts/pallas_call | solution.py:436
  39.0 0.6 %convert_element_type.3 = bf16[48,256]{1,0:T(8,128)(2,1)} convert(f32[48,256]{1,0:T(8,128)S(1)} %experts.1) | non-fusion elementwise | flops 12288 | bytes 73728 | tf_op jit(solution)/shard_map/convert_element_type | solution.py:466
